TPU v7x, 512 devices: a whole 4x8x8 slice. The times are simulated.
512 devices in a mesh: sp: 32 (over z, x), tp: 16 (over y, core).
Axes of the slice: x: 4, y: 8, z: 8, core: 2. Of those that a mesh axis runs over, the one named last changes fastest.
Arguments:
- skip_stream_entering: bfloat16 [4096, 2048], P('sp', 'tp'), may hold values from -24 to 24
- unfiltered_channel_feed: bfloat16 [4096, 2048], P('sp', 'tp'), may hold values from -6 to 6
- unfiltered_state_entry: bfloat16 [4096, 2048], P('sp', 'tp'), may hold values from -6 to 6
- unfiltered_state_exit: bfloat16 [4096, 2048], P('sp', 'tp'), may hold values from -6 to 6
- final_valve_preactivation: bfloat16 [4096, 2048], P('sp', 'tp'), may hold values from -6 to 6
- increment_preactivation: float32 [2, 32, 4096], P(None, 'tp', 'sp'), may hold values from -8 to 8
- summed_attenuation_both_ways: float32 [2, 32, 4096], P(None, 'tp', 'sp'), may hold values from -0.7 to 0, as said below
- channel_fading_speed: float32 [2, 32], P(None, 'tp'), may hold values from 4.8828125e-05 to 0.03, as said below
- channel_feed_filter: float32 [5, 2048], P(None, 'tp'), may hold values from -2.5 to 2.5
- state_entry_filter: float32 [5, 2048], P(None, 'tp'), may hold values from -2.5 to 2.5
- state_exit_filter: float32 [5, 2048], P(None, 'tp'), may hold values from -2.5 to 2.5
- clustered_rescale_factor: float32 [2048], P('tp'), may hold values from 0.1 to 1.9
- final_projection_weights: bfloat16 [2048, 2048], P(None, 'tp'), may hold values from -0.125 to 0.125
- specialist_rescale_factor: float32 [2048], replicated, may hold values from 0.1 to 1.9
- item_specialist_couple: int32 [4096, 2], P('sp'), may hold values from 0 to 31, all different within a row; in each aligned block of 128 rows (0 to 127, 128 to 255, ...) at most 16 rows name the same one
- selected_cluster_likelihood: float32 [4096], P('sp'), may hold values from 0.3 to 1
- selected_twin_scores_raw: float32 [4096, 2], P('sp'), may hold values from -6 to 6
- specialist_gating_weights: bfloat16 [32, 2048, 4096], P('sp', None, 'tp'), may hold values from -0.125 to 0.125
- specialist_raising_weights: bfloat16 [32, 2048, 4096], P('sp', None, 'tp'), may hold values from -0.125 to 0.125
- specialist_lowering_weights: bfloat16 [32, 4096, 2048], P('sp', 'tp'), may hold values from -0.09375 to 0.09375
Outputs:
- layer_out: bfloat16 [4096, 2048], P('sp', 'tp')
Inputs may be any that keep to these rules, and one draw needn't show every extreme that they name: For every head, dt times channel_fading_speed at the rate of the draw sets how far a state is carried; summed_attenuation_both_ways holds a few sharp losses of state. `summed_attenuation_both_ways`: mostly zero. `item_specialist_couple`: the two experts of a row differ. Among the rows of one index of sp (aligned blocks of 128 rows) no expert is named by more than 16 rows, a bound that some expert reaches in some blocks.
All inputs are finite; a program needn't handle non-finite values.
Results may differ from a plain program's by a relative error of at most 0.0095.
Values may be sent and summed in bfloat16 or wider, within the bound.
No kernel may reach another device: no remote copies, remote signals or barrier semaphores. Data moves between devices by JAX's collectives and lax.ppermute only.
A program may use at most 64 MiB of HBM per device.

v0:
```python
import jax
import jax.numpy as jnp
from jax import lax
from jax.sharding import Mesh
from jax.sharding import PartitionSpec as P

D = 2048
HD = 64
NS = 128
CONV = 5
SP = ("sp_0", "sp_1")
HIGHEST = lax.Precision.HIGHEST
group_eps = 1e-05
stream_eps = 1e-06


def extended(cells, sides, width):
    for axis, dim in sides:
        count = lax.axis_size(axis)
        ends = count - 1
        head = lax.slice_in_dim(cells, 0, width, axis=dim)
        tail = lax.slice_in_dim(cells, cells.shape[dim] - width, cells.shape[dim], axis=dim)
        cells = jnp.concatenate(
            [
                lax.ppermute(tail, axis, [(i, (i + 1) % count) for i in range(ends)]),
                cells,
                lax.ppermute(head, axis, [((i + 1) % count, i) for i in range(ends)]),
            ],
            axis=dim,
        )
    return cells


def filled_with(shard, identity):
    return jax.tree.map(
        lambda a, e: jnp.broadcast_to(jnp.asarray(e, a.dtype), a.shape), shard, identity
    )


def all_in_one(shard, axis):
    leaves = jax.tree.leaves(shard)
    sequence = sorted(range(len(leaves)), key=lambda k: -leaves[k].size)
    width = (1, *leaves[sequence[0]].shape)[-1]
    lines = [
        jnp.pad(leaves[k].reshape(-1), (0, -leaves[k].size % width)).reshape(-1, width)
        for k in sequence
    ]
    both, at, found = (lax.all_gather(jnp.concatenate(lines), axis), 0, {})
    for k, line in zip(sequence, lines):
        share = both[:, at : at + len(line)].reshape(len(both), -1)
        found[k] = share[:, : leaves[k].size].reshape(-1, *leaves[k].shape)
        at += len(line)
    numbers = iter(range(len(leaves)))
    return jax.tree.map(lambda _: found[next(numbers)], shard)


def carried_in(shard, axes, combine, identity, reverse):
    before = start = filled_with(shard, identity)
    so_far = shard
    for axis in reversed(axes):
        peers, mine = (lax.axis_size(axis), lax.axis_index(axis))
        pieces = all_in_one(
            jax.tree.map(
                lambda part, kind: part.astype(kind), so_far, (jnp.bfloat16, jnp.bfloat16)
            ),
            axis,
        )
        inside, so_far = (start, start)
        for k in reversed(range(peers)) if reverse else range(peers):
            passed = k > mine if reverse else k < mine
            so_far = combine(
                so_far, jax.tree.map(lambda part, own: part[k].astype(own.dtype), pieces, shard)
            )
            inside = jax.tree.map(lambda new, old: jnp.where(passed, new, old), so_far, inside)
        before = combine(inside, before)
    return before


def in_blocks(shard, dim, peers):
    shape = shard.shape
    parts = shard.reshape(*shape[:dim], peers, shape[dim] // peers, *shape[dim + 1 :])
    return jnp.moveaxis(parts, dim, 0)


def sum_at_owner(shard, axis, dim):
    peers = lax.axis_size(axis)
    parts = lax.all_to_all(in_blocks(shard, dim, peers), axis, 0, 0, tiled=True)
    return jnp.sum(parts.astype(jnp.float32), axis=0)


def block_parts(x_short, b_short, c_short, step_f, step_b, log_f, log_b):
    head_count = x_short.shape[1]
    group_count = b_short.shape[1]
    per_group = head_count // group_count
    length = x_short.shape[0]
    group_scores = jnp.einsum("tgn,sgn->gts", c_short, b_short, preferred_element_type=jnp.float32)
    x_block = x_short.astype(jnp.float32)
    b_block = b_short.astype(jnp.float32)
    c_block = c_short.astype(jnp.float32)
    scores = jnp.repeat(group_scores, per_group, axis=0)
    b_head = jnp.repeat(b_block, per_group, axis=1)
    c_head = jnp.repeat(c_block, per_group, axis=1)
    forward = jnp.cumsum(log_f, axis=1)
    backward = jnp.flip(jnp.cumsum(jnp.flip(log_b, 1), axis=1), 1)
    row_index = lax.broadcasted_iota(jnp.int32, (length, length), 0)
    col_index = lax.broadcasted_iota(jnp.int32, (length, length), 1)
    lower_mask = (col_index <= row_index)[None]
    upper_mask = (col_index >= row_index)[None]
    decay_fwd = jnp.where(
        lower_mask, jnp.exp(jnp.minimum(forward[:, :, None] - forward[:, None, :], 0.0)), 0.0
    )
    decay_bwd = jnp.where(
        upper_mask, jnp.exp(jnp.minimum(backward[:, :, None] - backward[:, None, :], 0.0)), 0.0
    )
    mixing = scores * (decay_fwd * step_f[:, None, :] + decay_bwd * step_b[:, None, :])
    within = jnp.einsum("hts,shp->thp", mixing, x_block, precision=HIGHEST)
    weight_fwd = jnp.exp(forward[:, -1:] - forward) * step_f
    weight_bwd = jnp.exp(backward[:, :1] - backward) * step_b
    state_fwd = jnp.einsum("hs,shp,shn->hpn", weight_fwd, x_block, b_head, precision=HIGHEST)
    state_bwd = jnp.einsum("hs,shp,shn->hpn", weight_bwd, x_block, b_head, precision=HIGHEST)
    return (
        within,
        state_fwd,
        state_bwd,
        forward[:, -1],
        backward[:, 0],
        jnp.exp(forward),
        jnp.exp(backward),
        c_head,
    )


def read_state(c_head, factor, state):
    return (
        jnp.einsum("thn,hpn->thp", c_head, state, precision=HIGHEST)
        * jnp.transpose(factor)[:, :, None]
    )


def compose(earlier, later):
    return (earlier[0] + later[0], earlier[1] * jnp.exp(later[0])[:, None, None] + later[1])


def body(
    skip_stream_entering,
    unfiltered_channel_feed,
    unfiltered_state_entry,
    unfiltered_state_exit,
    final_valve_preactivation,
    increment_preactivation,
    summed_attenuation_both_ways,
    channel_fading_speed,
    channel_feed_filter,
    state_entry_filter,
    state_exit_filter,
    clustered_rescale_factor,
    final_projection_weights,
    specialist_rescale_factor,
    item_specialist_couple,
    selected_cluster_likelihood,
    selected_twin_scores_raw,
    specialist_gating_weights,
    specialist_raising_weights,
    specialist_lowering_weights,
):
    tokens_here = skip_stream_entering.shape[0]
    heads_here = increment_preactivation.shape[1]
    x_width = unfiltered_channel_feed.shape[1]
    b_width = unfiltered_state_entry.shape[1]
    groups_here = b_width // NS
    joined = jnp.concatenate(
        [unfiltered_channel_feed, unfiltered_state_entry, unfiltered_state_exit], axis=1
    )
    padded = extended(joined, ((SP, 0),), CONV // 2)
    kernel = jnp.concatenate([channel_feed_filter, state_entry_filter, state_exit_filter], axis=1)
    summed = jnp.zeros(joined.shape, jnp.float32)
    for offset in range(CONV):
        summed = summed + kernel[offset] * padded[offset : offset + tokens_here].astype(jnp.float32)
    conv_out = jax.nn.silu(summed).astype(jnp.bfloat16)
    x_conv = conv_out[:, :x_width].reshape(tokens_here, heads_here, HD)
    b_conv = conv_out[:, x_width : x_width + b_width].reshape(tokens_here, groups_here, NS)
    c_conv = conv_out[:, x_width + b_width :].reshape(tokens_here, groups_here, NS)
    whole_increment_list = jax.nn.softplus(increment_preactivation)
    whole_attenuation_list = (
        -whole_increment_list * channel_fading_speed[:, :, None] + summed_attenuation_both_ways
    )
    within, state_fwd, state_bwd, total_fwd, total_bwd, factor_fwd, factor_bwd, c_head = (
        block_parts(
            x_conv,
            b_conv,
            c_conv,
            whole_increment_list[0],
            whole_increment_list[1],
            whole_attenuation_list[0],
            whole_attenuation_list[1],
        )
    )
    empty = (jnp.zeros_like(total_fwd), jnp.zeros_like(state_fwd))
    incoming_fwd = carried_in((total_fwd, state_fwd), SP, compose, empty, False)[1]
    incoming_bwd = carried_in((total_bwd, state_bwd), SP, compose, empty, True)[1]
    mixer_out = (
        within
        + read_state(c_head, factor_fwd, incoming_fwd)
        + read_state(c_head, factor_bwd, incoming_bwd)
    )
    gated = mixer_out.reshape(tokens_here, x_width) * jax.nn.silu(
        final_valve_preactivation.astype(jnp.float32)
    )
    grouped = gated.reshape(tokens_here, groups_here, -1)
    grouped = grouped * lax.rsqrt(jnp.mean(grouped * grouped, axis=-1, keepdims=True) + group_eps)
    mixed = (grouped.reshape(tokens_here, x_width) * clustered_rescale_factor).astype(jnp.bfloat16)
    projected = jnp.dot(
        lax.all_gather(mixed, "tp", axis=1, tiled=True),
        final_projection_weights,
        preferred_element_type=jnp.float32,
    )
    stream = (skip_stream_entering.astype(jnp.float32) + projected).astype(jnp.bfloat16)
    stream_f = stream.astype(jnp.float32)
    col_count = skip_stream_entering.shape[1]
    whole_rows = lax.all_gather(stream, "tp", axis=1, tiled=True).astype(jnp.float32)
    normal_rows = (
        whole_rows
        * lax.rsqrt(jnp.mean(whole_rows * whole_rows, axis=-1, keepdims=True) + stream_eps)
        * specialist_rescale_factor
    ).astype(jnp.bfloat16)
    expert_total = lax.axis_size(SP)
    capacity = 4 * tokens_here // expert_total
    flat_ids = item_specialist_couple.reshape(-1)
    assignments = flat_ids.shape[0]
    expert_iota = lax.broadcasted_iota(jnp.int32, (assignments, expert_total), 1)
    one_hot = (flat_ids[:, None] == expert_iota).astype(jnp.int32)
    ranking = jnp.sum((jnp.cumsum(one_hot, axis=0) - 1) * one_hot, axis=1)
    slot_index = flat_ids * capacity + ranking
    slot_iota = lax.broadcasted_iota(jnp.int32, (expert_total * capacity, assignments), 0)
    selector = (slot_index[None, :] == slot_iota).astype(jnp.bfloat16)
    selector = jnp.sum(selector.reshape(expert_total * capacity, tokens_here, -1), axis=2)
    weight_gate = specialist_gating_weights[0]
    weight_up = specialist_raising_weights[0]
    weight_down = specialist_lowering_weights[0]
    outgoing = jnp.dot(selector, normal_rows, preferred_element_type=jnp.float32).astype(
        jnp.bfloat16
    )
    outgoing = outgoing.reshape(expert_total, capacity, D)
    arrived = lax.all_to_all(outgoing, SP, split_axis=0, concat_axis=0, tiled=True)
    sources = arrived.shape[0]
    slot_count = arrived.shape[1]
    rows = arrived.reshape(sources * slot_count, arrived.shape[2])
    gate = jnp.dot(rows, weight_gate, preferred_element_type=jnp.float32)
    upward = jnp.dot(rows, weight_up, preferred_element_type=jnp.float32)
    hidden = (jax.nn.silu(gate) * upward).astype(jnp.bfloat16)
    partial_out = jnp.dot(hidden, weight_down, preferred_element_type=jnp.float32).astype(
        jnp.bfloat16
    )
    partial_out = partial_out.reshape(sources, slot_count, partial_out.shape[1])
    expert_cols = sum_at_owner(partial_out, "tp", 2).astype(jnp.bfloat16)
    returned = lax.all_to_all(expert_cols, SP, split_axis=0, concat_axis=0, tiled=True)
    flat_back = returned.reshape(expert_total * capacity, col_count)
    picked = (
        jnp.take(flat_back, slot_index, axis=0)
        .astype(jnp.float32)
        .reshape(tokens_here, -1, col_count)
    )
    first = jax.nn.sigmoid(selected_twin_scores_raw[:, 0] - selected_twin_scores_raw[:, 1])
    route_weight = selected_cluster_likelihood[:, None] * jnp.stack([first, 1.0 - first], axis=1)
    experts_sum = jnp.sum(route_weight[:, :, None] * picked, axis=1)
    return (stream_f + experts_sum).astype(jnp.bfloat16)


def solution(mesh):
    torus = Mesh(mesh.devices.reshape(8, 4, mesh.shape["tp"]), ("sp_0", "sp_1", "tp"))
    return jax.shard_map(
        body,
        mesh=torus,
        in_specs=(
            P(SP, "tp"),
            P(SP, "tp"),
            P(SP, "tp"),
            P(SP, "tp"),
            P(SP, "tp"),
            P(None, "tp", SP),
            P(None, "tp", SP),
            P(None, "tp"),
            P(None, "tp"),
            P(None, "tp"),
            P(None, "tp"),
            P("tp"),
            P(None, "tp"),
            P(),
            P(SP, None),
            P(SP),
            P(SP, None),
            P(SP, None, "tp"),
            P(SP, None, "tp"),
            P(SP, "tp", None),
        ),
        out_specs=P(SP, "tp"),
        check_vma=False,
    )
```

profile of v0, /device:TPU:1, one launch (start us, length us, event | category | flops | bytes accessed | tf_op | source)
XLA Modules:
  0.0 280.2 jit_solution(5651927392031734438)
XLA Ops:
  0.0 0.9 constant_dynamic-update-slice_fusion.5
  0.9 0.8 constant_dynamic-update-slice_fusion.4
  2.4 3.9 %collective-permute-start = (bf16[2,384]{1,0:T(2,128)(2,1)S(1)}, bf16[2,384]{1,0:T(2,128)(2,1)S(1)}, u32[]{:S(2)}, u32[]{:S(2)}) collective-permute-start(bf16[2,384]{1,0:T(2,128)(2,1)S(1)} %get-tuple-element.47), channel_id=1, source_target_pairs={{0,16},{16,32},{32,48},{48,64},{64,80},{80,96},{96,112},{112,128},... | collective-permute-start | bytes 4616 | tf_op jit(solution)/shard_map/ppermute | solution.py:25
  6.3 1.3 collective-permute-start.1
  7.7 0.8 copy.71
  8.8 0.8 multiply_add_fusion
  15.4 10.4 %all-gather.6 = bf16[4,129,128]{2,1,0:T(8,128)(2,1)S(1)} all-gather(bf16[1,129,128]{2,1,0:T(8,128)(2,1)S(1)} %maximum_bitcast_fusion.2), channel_id=4, replica_groups=mesh['sp_0'=8,'sp_1'=4,'tp'=16] {'sp_1'}, dimensions={0}, use_global_device_ids=true | all-gather | bytes 165120 | tf_op jit(solution)/shard_map/all_gather | solution.py:48
  26.6 27.4 %all-gather.7 = bf16[8,129,128]{2,1,0:T(8,128)(2,1)S(1)} all-gather(bf16[1,129,128]{2,1,0:T(8,128)(2,1)S(1)} %maximum_bitcast_fusion.3), channel_id=5, replica_groups=mesh['sp_0'=8,'sp_1'=4,'tp'=16] {'sp_0'}, dimensions={0}, use_global_device_ids=true | all-gather | bytes 297216 | tf_op jit(solution)/shard_map/all_gather | solution.py:48
  54.2 9.1 %all-gather.4 = bf16[4,129,128]{2,1,0:T(8,128)(2,1)S(1)} all-gather(bf16[1,129,128]{2,1,0:T(8,128)(2,1)S(1)} %maximum_bitcast_fusion), channel_id=2, replica_groups=mesh['sp_0'=8,'sp_1'=4,'tp'=16] {'sp_1'}, dimensions={0}, use_global_device_ids=true | all-gather | bytes 165120 | tf_op jit(solution)/shard_map/all_gather | solution.py:48
  64.2 18.5 %all-gather.5 = bf16[8,129,128]{2,1,0:T(8,128)(2,1)S(1)} all-gather(bf16[1,129,128]{2,1,0:T(8,128)(2,1)S(1)} %maximum_bitcast_fusion.1), channel_id=3, replica_groups=mesh['sp_0'=8,'sp_1'=4,'tp'=16] {'sp_0'}, dimensions={0}, use_global_device_ids=true | all-gather | bytes 297216 | tf_op jit(solution)/shard_map/all_gather | solution.py:48
  84.8 37.9 %all_gather.38 = bf16[128,2048]{1,0:T(8,128)(2,1)S(1)} all-gather(bf16[128,128]{1,0:T(8,128)(2,1)S(1)} %multiply_convert_fusion.1), channel_id=1, replica_groups=mesh['sp_0'=8,'sp_1'=4,'tp'=16] {'tp'}, dimensions={1}, use_global_device_ids=true | all-gather | bytes 557056 | tf_op jit(solution)/shard_map/all_gather | solution.py:213
  123.0 16.4 %all_gather.39 = bf16[128,2048]{1,0:T(8,128)(2,1)S(1)} all-gather(bf16[128,128]{1,0:T(8,128)(2,1)S(1)} %fusion.6), channel_id=1, replica_groups=mesh['sp_0'=8,'sp_1'=4,'tp'=16] {'tp'}, dimensions={1}, use_global_device_ids=true | all-gather | bytes 557056 | tf_op jit(solution)/shard_map/all_gather | solution.py:220
  139.6 0.8 convolution_convert_fusion.1
  140.4 55.6 %all_to_all.15 = bf16[32,16,2048]{2,1,0:T(8,128)(2,1)S(1)} all-to-all(bf16[32,16,2048]{2,1,0:T(8,128)(2,1)S(1)} %bitcast.252), channel_id=1, replica_groups=mesh['sp_0'=8,'sp_1'=4,'tp'=16] {'sp_0','sp_1'}, dimensions={0} | all-to-all | bytes 4194304 | tf_op jit(solution)/shard_map/all_to_all | solution.py:244
  196.0 1.5 fusion.12
  197.5 5.0 %fusion = bf16[64,8,16,128]{3,1,2,0:T(8,128)(2,1)} fusion(bf16[1,256,2048]{2,1,0:T(8,128)(2,1)S(1)} %copy-done, bf16[512,2048]{1,0:T(8,128)(2,1)S(1)} %bitcast.256, bf16[1,2048,256]{2,1,0:T(8,128)(2,1)} %param.38, f32[512,256]{1,0:T(8,128)} %fusion.12), kind=kOutput, calls=%fused_computation.4 | convolution fusion | flops 1075576832 | bytes 6815744 | tf_op jit(solution)/shard_map/dot_general | solution.py:251
  202.6 2.2 copy.83
  204.8 1.9 copy.90
  206.7 6.9 %all-to-all-start.1 = ((bf16[16,32,16,128]{3,2,1,0:T(8,128)(2,1)}), bf16[16,32,16,128]{3,2,1,0:T(8,128)(2,1)S(1)}, u32[]{:S(2)}, u32[]{:S(2)}) async-start(bf16[16,32,16,128]{3,2,1,0:T(8,128)(2,1)} %bitcast.251), calls=%async_computation.1 | async-start | bytes 4194304 | tf_op jit(solution)/shard_map/all_to_all | solution.py:87
  214.2 48.5 %all-to-all-done.1 = bf16[16,32,16,128]{3,2,1,0:T(8,128)(2,1)S(1)} async-done(((bf16[16,32,16,128]{3,2,1,0:T(8,128)(2,1)}), bf16[16,32,16,128]{3,2,1,0:T(8,128)(2,1)S(1)}, u32[]{:S(2)}, u32[]{:S(2)}) %all-to-all-start.1) | async-done | bytes 2097184 | tf_op jit(solution)/shard_map/all_to_all | solution.py:87
  262.6 0.9 reduce_sum.69
  263.6 5.3 %all-to-all-start.2 = ((bf16[32,16,128]{2,1,0:T(8,128)(2,1)}), bf16[32,16,128]{2,1,0:T(8,128)(2,1)S(1)}, u32[]{:S(2)}, u32[]{:S(2)}) async-start(bf16[32,16,128]{2,1,0:T(8,128)(2,1)} %reduce_sum.69), calls=%async_computation.2 | async-start | bytes 262144 | tf_op jit(solution)/shard_map/all_to_all | solution.py:256
  268.9 9.4 %all-to-all-done.2 = bf16[32,16,128]{2,1,0:T(8,128)(2,1)S(1)} async-done(((bf16[32,16,128]{2,1,0:T(8,128)(2,1)}), bf16[32,16,128]{2,1,0:T(8,128)(2,1)S(1)}, u32[]{:S(2)}, u32[]{:S(2)}) %all-to-all-start.2) | async-done | bytes 131104 | tf_op jit(solution)/shard_map/all_to_all | solution.py:256
  278.3 0.9 gather_fusion
  (122 shorter events, 12.6 us)
Async XLA Ops:
  0.0 197.5 %copy-start = (bf16[1,256,2048]{2,1,0:T(8,128)(2,1)S(1)}, bf16[1,256,2048]{2,1,0:T(8,128)(2,1)}, u32[]{:S(2)}) copy-start(bf16[1,256,2048]{2,1,0:T(8,128)(2,1)} %param.39) | copy-start | bytes 3145732
  2.4 12.4 %collective-permute-start = (bf16[2,384]{1,0:T(2,128)(2,1)S(1)}, bf16[2,384]{1,0:T(2,128)(2,1)S(1)}, u32[]{:S(2)}, u32[]{:S(2)}) collective-permute-start(bf16[2,384]{1,0:T(2,128)(2,1)S(1)} %get-tuple-element.47), channel_id=1, source_target_pairs={{0,16},{16,32},{32,48},{48,64},{64,80},{80,96},{96,112},{112,128},... | collective-permute-start | bytes 4616 | tf_op jit(solution)/shard_map/ppermute | solution.py:25
  6.3 8.4 %collective-permute-start.1 = (bf16[2,384]{1,0:T(2,128)(2,1)S(1)}, bf16[2,384]{1,0:T(2,128)(2,1)S(1)}, u32[]{:S(2)}, u32[]{:S(2)}) collective-permute-start(bf16[2,384]{1,0:T(2,128)(2,1)S(1)} %get-tuple-element.48), channel_id=1, source_target_pairs={{16,0},{32,16},{48,32},{64,48},{80,64},{96,80},{112,96},{128,112},... | collective-permute-start | bytes 4616 | tf_op jit(solution)/shard_map/ppermute | solution.py:27
  82.7 1.9 copy-start.2
  82.7 2.0 copy-start.7
  82.7 40.0 %copy-start.1 = (bf16[2048,128]{1,0:T(8,128)(2,1)S(1)}, bf16[2048,128]{1,0:T(8,128)(2,1)}, u32[]{:S(2)}) copy-start(bf16[2048,128]{1,0:T(8,128)(2,1)} %param.32) | copy-start | bytes 1572868
  82.7 40.0 %copy-start.3 = (bf16[128,128]{1,0:T(8,128)(2,1)S(1)}, bf16[128,128]{1,0:T(8,128)(2,1)}, u32[]{:S(2)}) copy-start(bf16[128,128]{1,0:T(8,128)(2,1)} %param.20) | copy-start | bytes 98308
  83.9 55.7 %copy-start.5 = (f32[2048]{0:T(1024)S(1)}, f32[2048]{0:T(1024)}, u32[]{:S(2)}) copy-start(f32[2048]{0:T(1024)} %param.33) | copy-start | bytes 24580
  140.4 55.6 %copy-start.9 = (bf16[1,2048,256]{2,1,0:T(8,128)(2,1)S(1)}, bf16[1,2048,256]{2,1,0:T(8,128)(2,1)}, u32[]{:S(2)}) copy-start(bf16[1,2048,256]{2,1,0:T(8,128)(2,1)} %param.37) | copy-start | bytes 3145732
  206.7 6.9 %copy-start.4 = (s32[128,2]{0,1:T(2,128)S(1)}, s32[128,2]{0,1:T(2,128)}, u32[]{:S(2)}) copy-start(s32[128,2]{0,1:T(2,128)} %param.34) | copy-start | bytes 3076
  206.7 7.3 %copy-start.6 = (f32[128,2]{0,1:T(2,128)S(1)}, f32[128,2]{0,1:T(2,128)}, u32[]{:S(2)}) copy-start(f32[128,2]{0,1:T(2,128)} %param.36) | copy-start | bytes 3076
  206.7 7.4 %copy-start.8 = (f32[128]{0:T(128)S(1)}, f32[128]{0:T(128)}, u32[]{:S(2)}) copy-start(f32[128]{0:T(128)} %param.35) | copy-start | bytes 1540
  206.7 56.0 %all-to-all-start.1 = ((bf16[16,32,16,128]{3,2,1,0:T(8,128)(2,1)}), bf16[16,32,16,128]{3,2,1,0:T(8,128)(2,1)S(1)}, u32[]{:S(2)}, u32[]{:S(2)}) async-start(bf16[16,32,16,128]{3,2,1,0:T(8,128)(2,1)} %bitcast.251), calls=%async_computation.1 | async-start | bytes 4194304 | tf_op jit(solution)/shard_map/all_to_all | solution.py:87
  263.6 14.8 %all-to-all-start.2 = ((bf16[32,16,128]{2,1,0:T(8,128)(2,1)}), bf16[32,16,128]{2,1,0:T(8,128)(2,1)S(1)}, u32[]{:S(2)}, u32[]{:S(2)}) async-start(bf16[32,16,128]{2,1,0:T(8,128)(2,1)} %reduce_sum.69), calls=%async_computation.2 | async-start | bytes 262144 | tf_op jit(solution)/shard_map/all_to_all | solution.py:256
where the time goes:
time: 281 us; the launch traced here: 280 us
  blocking collectives  175 us (62%)
  waiting for transfers between devices  57.9 us (21%)
  starting transfers between devices  17.4 us (6%)
  local copies, waits for them, and re-layouts  13.4 us (5%)
  matrix products  9.61 us (3%)
  other arithmetic  6.01 us (2%)
    all_gather x4, blocking collectives, all_in_one(): both, at, found = (lax.all_gather(jnp.concatenate(lines), axis), 0, {})  65.3 us
    all_to_all x1, blocking collectives, body(): lax.all_to_all(outgoing, SP, split_axis=0, concat_axis=0, tiled=True)  55.6 us
    all_to_all x1, waiting for transfers between devices, sum_at_owner(): parts = lax.all_to_all(in_blocks(shard, dim, peers), axis, 0, 0, tiled=True)  48.5 us
    all_gather x1, blocking collectives, body(): lax.all_gather(mixed, 'tp', axis=1, tiled=True)  37.9 us
    all_gather x1, blocking collectives, body(): lax.all_gather(stream, 'tp', axis=1, tiled=True).astype(jnp.float32)  16.4 us
    all_to_all x1, waiting for transfers between devices, body(): lax.all_to_all(expert_cols, SP, split_axis=0, concat_axis=0, tiled=True)  9.43 us
    all_to_all x1, starting transfers between devices, sum_at_owner(): parts = lax.all_to_all(in_blocks(shard, dim, peers), axis, 0, 0, tiled=True)  6.91 us
    unnamed x30, local copies, waits for them, and re-layouts  6.06 us
  transfers between devices with their start and end apart: 4, of which 2 were waited for; matrix products, arithmetic and copies ran while one was open for 3% of the time, Pallas kernels for 0%

commit v1 on v0

--- a/solution.py
+++ b/solution.py
@@ -1,8 +1,10 @@
+import functools
 import jax
 import jax.numpy as jnp
 from jax import lax
 from jax.sharding import Mesh
 from jax.sharding import PartitionSpec as P
+from jax.lax import axis_index, axis_size, ppermute
 
 D = 2048
 HD = 64
@@ -12,6 +14,31 @@
 HIGHEST = lax.Precision.HIGHEST
 group_eps = 1e-05
 stream_eps = 1e-06
+
+
+def advance_the_sheet(tile_in, at_axis):
+    h_now = list(tile_in.shape[1:])
+    h_now[at_axis] *= tile_in.shape[0]
+    return jnp.moveaxis(tile_in, 0, at_axis).reshape(h_now)
+
+
+def balance_heaps(arr_in, across, array_axis):
+    nodes = axis_size(across)
+    inbox = [(tick, (tick + 1) % nodes) for tick in range(nodes)]
+    tray = [(ix, p) for p, ix in inbox]
+    tmp, finding = ([], [])
+    for hop_no in range(nodes - 1):
+        if hop_no % 2 == 0:
+            tmp.append(ppermute(tmp[-1] if tmp else arr_in, across, inbox))
+        else:
+            finding.append(ppermute(finding[-1] if finding else arr_in, across, tray))
+    outer = jnp.stack([*tmp[::-1], arr_in, *finding], 0)
+    w2 = axis_index(across) - len(tmp)
+    outer = outer[(jnp.arange(nodes) - w2) % nodes]
+    return advance_the_sheet(outer, array_axis)
+
+
+loops_keep_up = functools.partial(balance_heaps, across="tp", array_axis=1)
 
 
 def extended(cells, sides, width):
@@ -210,9 +237,7 @@
     grouped = grouped * lax.rsqrt(jnp.mean(grouped * grouped, axis=-1, keepdims=True) + group_eps)
     mixed = (grouped.reshape(tokens_here, x_width) * clustered_rescale_factor).astype(jnp.bfloat16)
     projected = jnp.dot(
-        lax.all_gather(mixed, "tp", axis=1, tiled=True),
-        final_projection_weights,
-        preferred_element_type=jnp.float32,
+        loops_keep_up(mixed), final_projection_weights, preferred_element_type=jnp.float32
     )
     stream = (skip_stream_entering.astype(jnp.float32) + projected).astype(jnp.bfloat16)
     stream_f = stream.astype(jnp.float32)

time: 281 us -> 299 us (1.064)
  starting transfers between devices: 17.4 us -> 63.1 us
  blocking collectives: 175 us -> 142 us
  waiting for transfers between devices: 57.9 us -> 64.3 us
    ppermute x0 -> x15, starting transfers between devices: none -> 43.8 us  [the longest x8 26.1 us: balance_heaps(): tmp.append(ppermute(tmp[-1] if tmp else arr_in, across, inbox))]
    all_gather x1 -> x0, blocking collectives: 37.9 us -> none  [body(): lax.all_gather(mixed, 'tp', axis=1, tiled=True)]
    ppermute x0 -> x15, waiting for transfers between devices: none -> 6.33 us  [the longest x7 4.58 us: balance_heaps(): finding.append(ppermute(finding[-1] if finding else arr_in, across, tray))]
    all_gather x1, blocking collectives: 16.4 us -> 20.2 us  [body(): lax.all_gather(stream, 'tp', axis=1, tiled=True).astype(jnp.float32)]
    unnamed x30 -> x45, local copies, waits for them, and re-layouts: 6.06 us -> 5.53 us
  transfers between devices with their start and end apart: 4 -> 19, of which waited for: 2 -> 17; matrix products, arithmetic and copies ran while one was open for 3% -> 2% of each run, Pallas kernels for 0% -> 0%
where the time goes in v1:
time: 299 us; the launch traced here: 298 us
  blocking collectives  142 us (47%)
  waiting for transfers between devices  64.3 us (22%)
  starting transfers between devices  63.1 us (21%)
  local copies, waits for them, and re-layouts  13.9 us (5%)
  matrix products  9.68 us (3%)
  other arithmetic  5.31 us (2%)
    all_gather x4, blocking collectives, all_in_one(): both, at, found = (lax.all_gather(jnp.concatenate(lines), axis), 0, {})  65.6 us
    all_to_all x1, blocking collectives, body(): lax.all_to_all(outgoing, SP, split_axis=0, concat_axis=0, tiled=True)  55.7 us
    all_to_all x1, waiting for transfers between devices, sum_at_owner(): parts = lax.all_to_all(in_blocks(shard, dim, peers), axis, 0, 0, tiled=True)  48.5 us
    ppermute x8, starting transfers between devices, balance_heaps(): tmp.append(ppermute(tmp[-1] if tmp else arr_in, across, inbox))  26.1 us
    all_gather x1, blocking collectives, body(): lax.all_gather(stream, 'tp', axis=1, tiled=True).astype(jnp.float32)  20.2 us
    ppermute x7, starting transfers between devices, balance_heaps(): finding.append(ppermute(finding[-1] if finding else arr_in, across, tray))  17.7 us
    all_to_all x1, waiting for transfers between devices, body(): lax.all_to_all(expert_cols, SP, split_axis=0, concat_axis=0, tiled=True)  9.43 us
    all_to_all x1, starting transfers between devices, sum_at_owner(): parts = lax.all_to_all(in_blocks(shard, dim, peers), axis, 0, 0, tiled=True)  8.68 us
  transfers between devices with their start and end apart: 19, of which 17 were waited for; matrix products, arithmetic and copies ran while one was open for 2% of the time, Pallas kernels for 0%

profile of v1, /device:TPU:1, one launch (start us, length us, event | category | flops | bytes accessed | tf_op | source)
XLA Modules:
  0.0 298.4 jit_solution(8768866199745308086)
XLA Ops:
  2.4 3.9 %collective-permute-start = (bf16[2,384]{1,0:T(2,128)(2,1)S(1)}, bf16[2,384]{1,0:T(2,128)(2,1)S(1)}, u32[]{:S(2)}, u32[]{:S(2)}) collective-permute-start(bf16[2,384]{1,0:T(2,128)(2,1)S(1)} %get-tuple-element.47), channel_id=1, source_target_pairs={{0,16},{16,32},{32,48},{48,64},{64,80},{80,96},{96,112},{112,128},... | collective-permute-start | bytes 4616 | tf_op jit(solution)/shard_map/ppermute | solution.py:52
  12.4 10.7 %all-gather.6 = bf16[4,129,128]{2,1,0:T(8,128)(2,1)S(1)} all-gather(bf16[1,129,128]{2,1,0:T(8,128)(2,1)S(1)} %maximum_bitcast_fusion.2), channel_id=4, replica_groups=mesh['sp_0'=8,'sp_1'=4,'tp'=16] {'sp_1'}, dimensions={0}, use_global_device_ids=true | all-gather | bytes 165120 | tf_op jit(solution)/shard_map/all_gather | solution.py:75
  23.9 27.0 %all-gather.7 = bf16[8,129,128]{2,1,0:T(8,128)(2,1)S(1)} all-gather(bf16[1,129,128]{2,1,0:T(8,128)(2,1)S(1)} %maximum_bitcast_fusion.3), channel_id=5, replica_groups=mesh['sp_0'=8,'sp_1'=4,'tp'=16] {'sp_0'}, dimensions={0}, use_global_device_ids=true | all-gather | bytes 297216 | tf_op jit(solution)/shard_map/all_gather | solution.py:75
  51.2 9.1 %all-gather.4 = bf16[4,129,128]{2,1,0:T(8,128)(2,1)S(1)} all-gather(bf16[1,129,128]{2,1,0:T(8,128)(2,1)S(1)} %maximum_bitcast_fusion), channel_id=2, replica_groups=mesh['sp_0'=8,'sp_1'=4,'tp'=16] {'sp_1'}, dimensions={0}, use_global_device_ids=true | all-gather | bytes 165120 | tf_op jit(solution)/shard_map/all_gather | solution.py:75
  61.2 18.8 %all-gather.5 = bf16[8,129,128]{2,1,0:T(8,128)(2,1)S(1)} all-gather(bf16[1,129,128]{2,1,0:T(8,128)(2,1)S(1)} %maximum_bitcast_fusion.1), channel_id=3, replica_groups=mesh['sp_0'=8,'sp_1'=4,'tp'=16] {'sp_0'}, dimensions={0}, use_global_device_ids=true | all-gather | bytes 297216 | tf_op jit(solution)/shard_map/all_gather | solution.py:75
  82.1 19.9 %collective-permute-start.2 = (bf16[128,128]{1,0:T(8,128)(2,1)S(1)}, bf16[128,128]{1,0:T(8,128)(2,1)S(1)}, u32[]{:S(2)}, u32[]{:S(2)}) collective-permute-start(bf16[128,128]{1,0:T(8,128)(2,1)S(1)} %multiply_convert_fusion.1), channel_id=1, source_target_pairs={{0,1},{1,2},{2,3},{3,4},{4,5},{5,6},{6,7},{7,8},{8,9},{9,10},{10,1... | collective-permute-start | bytes 98312 | tf_op jit(solution)/shard_map/ppermute | solution.py:32
  103.0 2.3 collective-permute-start.3
  106.3 2.3 collective-permute-start.4
  110.6 1.4 collective-permute-start.5
  112.8 2.2 collective-permute-start.12
  116.2 3.4 %collective-permute-start.13 = (bf16[128,128]{1,0:T(8,128)(2,1)S(1)}, bf16[128,128]{1,0:T(8,128)(2,1)S(1)}, u32[]{:S(2)}, u32[]{:S(2)}) collective-permute-start(bf16[128,128]{1,0:T(8,128)(2,1)S(1)} %collective-permute-done.12), channel_id=1, source_target_pairs={{1,0},{2,1},{3,2},{4,3},{5,4},{6,5},{7,6},{8,7},{9,8},{10,9},{11,1... | collective-permute-start | bytes 98312 | tf_op jit(solution)/shard_map/ppermute | solution.py:34
  120.5 3.7 %collective-permute-start.14 = (bf16[128,128]{1,0:T(8,128)(2,1)S(1)}, bf16[128,128]{1,0:T(8,128)(2,1)S(1)}, u32[]{:S(2)}, u32[]{:S(2)}) collective-permute-start(bf16[128,128]{1,0:T(8,128)(2,1)S(1)} %collective-permute-done.13), channel_id=1, source_target_pairs={{1,0},{2,1},{3,2},{4,3},{5,4},{6,5},{7,6},{8,7},{9,8},{10,9},{11,1... | collective-permute-start | bytes 98312 | tf_op jit(solution)/shard_map/ppermute | solution.py:34
  125.0 3.7 %collective-permute-start.15 = (bf16[128,128]{1,0:T(8,128)(2,1)S(1)}, bf16[128,128]{1,0:T(8,128)(2,1)S(1)}, u32[]{:S(2)}, u32[]{:S(2)}) collective-permute-start(bf16[128,128]{1,0:T(8,128)(2,1)S(1)} %collective-permute-done.14), channel_id=1, source_target_pairs={{1,0},{2,1},{3,2},{4,3},{5,4},{6,5},{7,6},{8,7},{9,8},{10,9},{11,1... | collective-permute-start | bytes 98312 | tf_op jit(solution)/shard_map/ppermute | solution.py:34
  129.6 3.7 %collective-permute-start.16 = (bf16[128,128]{1,0:T(8,128)(2,1)S(1)}, bf16[128,128]{1,0:T(8,128)(2,1)S(1)}, u32[]{:S(2)}, u32[]{:S(2)}) collective-permute-start(bf16[128,128]{1,0:T(8,128)(2,1)S(1)} %collective-permute-done.15), channel_id=1, source_target_pairs={{1,0},{2,1},{3,2},{4,3},{5,4},{6,5},{7,6},{8,7},{9,8},{10,9},{11,1... | collective-permute-start | bytes 98312 | tf_op jit(solution)/shard_map/ppermute | solution.py:34
  135.5 20.2 %all_gather.35 = bf16[128,2048]{1,0:T(8,128)(2,1)S(1)} all-gather(bf16[128,128]{1,0:T(8,128)(2,1)S(1)} %fusion.6), channel_id=1, replica_groups=mesh['sp_0'=8,'sp_1'=4,'tp'=16] {'tp'}, dimensions={1}, use_global_device_ids=true | all-gather | bytes 557056 | tf_op jit(solution)/shard_map/all_gather | solution.py:245
  156.7 55.7 %all_to_all.15 = bf16[32,16,2048]{2,1,0:T(8,128)(2,1)S(1)} all-to-all(bf16[32,16,2048]{2,1,0:T(8,128)(2,1)S(1)} %bitcast.288), channel_id=1, replica_groups=mesh['sp_0'=8,'sp_1'=4,'tp'=16] {'sp_0','sp_1'}, dimensions={0} | all-to-all | bytes 4194304 | tf_op jit(solution)/shard_map/all_to_all | solution.py:269
  212.4 1.5 fusion.12
  214.0 5.0 %fusion = bf16[64,8,16,128]{3,1,2,0:T(8,128)(2,1)} fusion(bf16[1,256,2048]{2,1,0:T(8,128)(2,1)S(1)} %copy-done, bf16[512,2048]{1,0:T(8,128)(2,1)S(1)} %bitcast.292, bf16[1,2048,256]{2,1,0:T(8,128)(2,1)} %param.38, f32[512,256]{1,0:T(8,128)} %fusion.12), kind=kOutput, calls=%fused_computation.5 | convolution fusion | flops 1075576832 | bytes 6815744 | tf_op jit(solution)/shard_map/dot_general | solution.py:276
  219.0 2.2 copy.87
  221.2 1.9 copy.94
  223.1 8.7 %all-to-all-start.1 = ((bf16[16,32,16,128]{3,2,1,0:T(8,128)(2,1)}), bf16[16,32,16,128]{3,2,1,0:T(8,128)(2,1)S(1)}, u32[]{:S(2)}, u32[]{:S(2)}) async-start(bf16[16,32,16,128]{3,2,1,0:T(8,128)(2,1)} %bitcast.287), calls=%async_computation.1 | async-start | bytes 4194304 | tf_op jit(solution)/shard_map/all_to_all | solution.py:114
  232.3 48.5 %all-to-all-done.1 = bf16[16,32,16,128]{3,2,1,0:T(8,128)(2,1)S(1)} async-done(((bf16[16,32,16,128]{3,2,1,0:T(8,128)(2,1)}), bf16[16,32,16,128]{3,2,1,0:T(8,128)(2,1)S(1)}, u32[]{:S(2)}, u32[]{:S(2)}) %all-to-all-start.1) | async-done | bytes 2097184 | tf_op jit(solution)/shard_map/all_to_all | solution.py:114
  281.8 5.3 %all-to-all-start.2 = ((bf16[32,16,128]{2,1,0:T(8,128)(2,1)}), bf16[32,16,128]{2,1,0:T(8,128)(2,1)S(1)}, u32[]{:S(2)}, u32[]{:S(2)}) async-start(bf16[32,16,128]{2,1,0:T(8,128)(2,1)} %reduce_sum.69), calls=%async_computation.2 | async-start | bytes 262144 | tf_op jit(solution)/shard_map/all_to_all | solution.py:281
  287.1 9.4 %all-to-all-done.2 = bf16[32,16,128]{2,1,0:T(8,128)(2,1)S(1)} async-done(((bf16[32,16,128]{2,1,0:T(8,128)(2,1)}), bf16[32,16,128]{2,1,0:T(8,128)(2,1)S(1)}, u32[]{:S(2)}, u32[]{:S(2)}) %all-to-all-start.2) | async-done | bytes 131104 | tf_op jit(solution)/shard_map/all_to_all | solution.py:281
  (171 shorter events, 27.1 us)
Async XLA Ops:
  0.0 214.0 %copy-start = (bf16[1,256,2048]{2,1,0:T(8,128)(2,1)S(1)}, bf16[1,256,2048]{2,1,0:T(8,128)(2,1)}, u32[]{:S(2)}) copy-start(bf16[1,256,2048]{2,1,0:T(8,128)(2,1)} %param.39) | copy-start | bytes 3145732
  2.4 9.4 %collective-permute-start = (bf16[2,384]{1,0:T(2,128)(2,1)S(1)}, bf16[2,384]{1,0:T(2,128)(2,1)S(1)}, u32[]{:S(2)}, u32[]{:S(2)}) collective-permute-start(bf16[2,384]{1,0:T(2,128)(2,1)S(1)} %get-tuple-element.47), channel_id=1, source_target_pairs={{0,16},{16,32},{32,48},{48,64},{64,80},{80,96},{96,112},{112,128},... | collective-permute-start | bytes 4616 | tf_op jit(solution)/shard_map/ppermute | solution.py:52
  6.3 5.5 %collective-permute-start.1 = (bf16[2,384]{1,0:T(2,128)(2,1)S(1)}, bf16[2,384]{1,0:T(2,128)(2,1)S(1)}, u32[]{:S(2)}, u32[]{:S(2)}) collective-permute-start(bf16[2,384]{1,0:T(2,128)(2,1)S(1)} %get-tuple-element.48), channel_id=1, source_target_pairs={{16,0},{32,16},{48,32},{64,48},{80,64},{96,80},{112,96},{128,112},... | collective-permute-start | bytes 4616 | tf_op jit(solution)/shard_map/ppermute | solution.py:54
  80.0 22.0 %copy-start.4 = (s32[128,2]{0,1:T(2,128)S(1)}, s32[128,2]{0,1:T(2,128)}, u32[]{:S(2)}) copy-start(s32[128,2]{0,1:T(2,128)} %param.34) | copy-start | bytes 3076
  81.7 53.4 %copy-start.1 = (bf16[2048,128]{1,0:T(8,128)(2,1)S(1)}, bf16[2048,128]{1,0:T(8,128)(2,1)}, u32[]{:S(2)}) copy-start(bf16[2048,128]{1,0:T(8,128)(2,1)} %param.32) | copy-start | bytes 1572868
  81.7 53.4 %copy-start.3 = (bf16[128,128]{1,0:T(8,128)(2,1)S(1)}, bf16[128,128]{1,0:T(8,128)(2,1)}, u32[]{:S(2)}) copy-start(bf16[128,128]{1,0:T(8,128)(2,1)} %param.20) | copy-start | bytes 98308
  82.1 20.9 %collective-permute-start.2 = (bf16[128,128]{1,0:T(8,128)(2,1)S(1)}, bf16[128,128]{1,0:T(8,128)(2,1)S(1)}, u32[]{:S(2)}, u32[]{:S(2)}) collective-permute-start(bf16[128,128]{1,0:T(8,128)(2,1)S(1)} %multiply_convert_fusion.1), channel_id=1, source_target_pairs={{0,1},{1,2},{2,3},{3,4},{4,5},{5,6},{6,7},{7,8},{8,9},{9,10},{10,1... | collective-permute-start | bytes 98312 | tf_op jit(solution)/shard_map/ppermute | solution.py:32
  103.0 3.3 %collective-permute-start.3 = (bf16[128,128]{1,0:T(8,128)(2,1)S(1)}, bf16[128,128]{1,0:T(8,128)(2,1)S(1)}, u32[]{:S(2)}, u32[]{:S(2)}) collective-permute-start(bf16[128,128]{1,0:T(8,128)(2,1)S(1)} %collective-permute-done.2), channel_id=1, source_target_pairs={{0,1},{1,2},{2,3},{3,4},{4,5},{5,6},{6,7},{7,8},{8,9},{9,10},{10,1... | collective-permute-start | bytes 98312 | tf_op jit(solution)/shard_map/ppermute | solution.py:32
  105.9 3.6 %collective-permute-start.10 = (bf16[128,128]{1,0:T(8,128)(2,1)S(1)}, bf16[128,128]{1,0:T(8,128)(2,1)S(1)}, u32[]{:S(2)}, u32[]{:S(2)}) collective-permute-start(bf16[128,128]{1,0:T(8,128)(2,1)S(1)} %multiply_convert_fusion.1), channel_id=1, source_target_pairs={{1,0},{2,1},{3,2},{4,3},{5,4},{6,5},{7,6},{8,7},{9,8},{10,9},{11,1... | collective-permute-start | bytes 98312 | tf_op jit(solution)/shard_map/ppermute | solution.py:34
  106.3 4.3 %collective-permute-start.4 = (bf16[128,128]{1,0:T(8,128)(2,1)S(1)}, bf16[128,128]{1,0:T(8,128)(2,1)S(1)}, u32[]{:S(2)}, u32[]{:S(2)}) collective-permute-start(bf16[128,128]{1,0:T(8,128)(2,1)S(1)} %collective-permute-done.3), channel_id=1, source_target_pairs={{0,1},{1,2},{2,3},{3,4},{4,5},{5,6},{6,7},{7,8},{8,9},{9,10},{10,1... | collective-permute-start | bytes 98312 | tf_op jit(solution)/shard_map/ppermute | solution.py:32
  109.5 3.3 %collective-permute-start.11 = (bf16[128,128]{1,0:T(8,128)(2,1)S(1)}, bf16[128,128]{1,0:T(8,128)(2,1)S(1)}, u32[]{:S(2)}, u32[]{:S(2)}) collective-permute-start(bf16[128,128]{1,0:T(8,128)(2,1)S(1)} %collective-permute-done.10), channel_id=1, source_target_pairs={{1,0},{2,1},{3,2},{4,3},{5,4},{6,5},{7,6},{8,7},{9,8},{10,9},{11,1... | collective-permute-start | bytes 98312 | tf_op jit(solution)/shard_map/ppermute | solution.py:34
  110.6 4.6 %collective-permute-start.5 = (bf16[128,128]{1,0:T(8,128)(2,1)S(1)}, bf16[128,128]{1,0:T(8,128)(2,1)S(1)}, u32[]{:S(2)}, u32[]{:S(2)}) collective-permute-start(bf16[128,128]{1,0:T(8,128)(2,1)S(1)} %collective-permute-done.4), channel_id=1, source_target_pairs={{0,1},{1,2},{2,3},{3,4},{4,5},{5,6},{6,7},{7,8},{8,9},{9,10},{10,1... | collective-permute-start | bytes 98312 | tf_op jit(solution)/shard_map/ppermute | solution.py:32
  112.8 3.3 %collective-permute-start.12 = (bf16[128,128]{1,0:T(8,128)(2,1)S(1)}, bf16[128,128]{1,0:T(8,128)(2,1)S(1)}, u32[]{:S(2)}, u32[]{:S(2)}) collective-permute-start(bf16[128,128]{1,0:T(8,128)(2,1)S(1)} %collective-permute-done.11), channel_id=1, source_target_pairs={{1,0},{2,1},{3,2},{4,3},{5,4},{6,5},{7,6},{8,7},{9,8},{10,9},{11,1... | collective-permute-start | bytes 98312 | tf_op jit(solution)/shard_map/ppermute | solution.py:34
  115.1 4.6 %collective-permute-start.6 = (bf16[128,128]{1,0:T(8,128)(2,1)S(1)}, bf16[128,128]{1,0:T(8,128)(2,1)S(1)}, u32[]{:S(2)}, u32[]{:S(2)}) collective-permute-start(bf16[128,128]{1,0:T(8,128)(2,1)S(1)} %collective-permute-done.5), channel_id=1, source_target_pairs={{0,1},{1,2},{2,3},{3,4},{4,5},{5,6},{6,7},{7,8},{8,9},{9,10},{10,1... | collective-permute-start | bytes 98312 | tf_op jit(solution)/shard_map/ppermute | solution.py:32
  116.2 4.3 %collective-permute-start.13 = (bf16[128,128]{1,0:T(8,128)(2,1)S(1)}, bf16[128,128]{1,0:T(8,128)(2,1)S(1)}, u32[]{:S(2)}, u32[]{:S(2)}) collective-permute-start(bf16[128,128]{1,0:T(8,128)(2,1)S(1)} %collective-permute-done.12), channel_id=1, source_target_pairs={{1,0},{2,1},{3,2},{4,3},{5,4},{6,5},{7,6},{8,7},{9,8},{10,9},{11,1... | collective-permute-start | bytes 98312 | tf_op jit(solution)/shard_map/ppermute | solution.py:34
  119.7 4.6 %collective-permute-start.7 = (bf16[128,128]{1,0:T(8,128)(2,1)S(1)}, bf16[128,128]{1,0:T(8,128)(2,1)S(1)}, u32[]{:S(2)}, u32[]{:S(2)}) collective-permute-start(bf16[128,128]{1,0:T(8,128)(2,1)S(1)} %collective-permute-done.6), channel_id=1, source_target_pairs={{0,1},{1,2},{2,3},{3,4},{4,5},{5,6},{6,7},{7,8},{8,9},{9,10},{10,1... | collective-permute-start | bytes 98312 | tf_op jit(solution)/shard_map/ppermute | solution.py:32
  120.5 4.6 %collective-permute-start.14 = (bf16[128,128]{1,0:T(8,128)(2,1)S(1)}, bf16[128,128]{1,0:T(8,128)(2,1)S(1)}, u32[]{:S(2)}, u32[]{:S(2)}) collective-permute-start(bf16[128,128]{1,0:T(8,128)(2,1)S(1)} %collective-permute-done.13), channel_id=1, source_target_pairs={{1,0},{2,1},{3,2},{4,3},{5,4},{6,5},{7,6},{8,7},{9,8},{10,9},{11,1... | collective-permute-start | bytes 98312 | tf_op jit(solution)/shard_map/ppermute | solution.py:34
  124.2 4.6 %collective-permute-start.8 = (bf16[128,128]{1,0:T(8,128)(2,1)S(1)}, bf16[128,128]{1,0:T(8,128)(2,1)S(1)}, u32[]{:S(2)}, u32[]{:S(2)}) collective-permute-start(bf16[128,128]{1,0:T(8,128)(2,1)S(1)} %collective-permute-done.7), channel_id=1, source_target_pairs={{0,1},{1,2},{2,3},{3,4},{4,5},{5,6},{6,7},{7,8},{8,9},{9,10},{10,1... | collective-permute-start | bytes 98312 | tf_op jit(solution)/shard_map/ppermute | solution.py:32
  125.0 4.6 %collective-permute-start.15 = (bf16[128,128]{1,0:T(8,128)(2,1)S(1)}, bf16[128,128]{1,0:T(8,128)(2,1)S(1)}, u32[]{:S(2)}, u32[]{:S(2)}) collective-permute-start(bf16[128,128]{1,0:T(8,128)(2,1)S(1)} %collective-permute-done.14), channel_id=1, source_target_pairs={{1,0},{2,1},{3,2},{4,3},{5,4},{6,5},{7,6},{8,7},{9,8},{10,9},{11,1... | collective-permute-start | bytes 98312 | tf_op jit(solution)/shard_map/ppermute | solution.py:34
  128.8 4.6 %collective-permute-start.9 = (bf16[128,128]{1,0:T(8,128)(2,1)S(1)}, bf16[128,128]{1,0:T(8,128)(2,1)S(1)}, u32[]{:S(2)}, u32[]{:S(2)}) collective-permute-start(bf16[128,128]{1,0:T(8,128)(2,1)S(1)} %collective-permute-done.8), channel_id=1, source_target_pairs={{0,1},{1,2},{2,3},{3,4},{4,5},{5,6},{6,7},{7,8},{8,9},{9,10},{10,1... | collective-permute-start | bytes 98312 | tf_op jit(solution)/shard_map/ppermute | solution.py:32
  129.6 4.6 %collective-permute-start.16 = (bf16[128,128]{1,0:T(8,128)(2,1)S(1)}, bf16[128,128]{1,0:T(8,128)(2,1)S(1)}, u32[]{:S(2)}, u32[]{:S(2)}) collective-permute-start(bf16[128,128]{1,0:T(8,128)(2,1)S(1)} %collective-permute-done.15), channel_id=1, source_target_pairs={{1,0},{2,1},{3,2},{4,3},{5,4},{6,5},{7,6},{8,7},{9,8},{10,9},{11,1... | collective-permute-start | bytes 98312 | tf_op jit(solution)/shard_map/ppermute | solution.py:34
  156.7 55.7 %copy-start.9 = (bf16[1,2048,256]{2,1,0:T(8,128)(2,1)S(1)}, bf16[1,2048,256]{2,1,0:T(8,128)(2,1)}, u32[]{:S(2)}) copy-start(bf16[1,2048,256]{2,1,0:T(8,128)(2,1)} %param.37) | copy-start | bytes 3145732
  223.1 57.7 %all-to-all-start.1 = ((bf16[16,32,16,128]{3,2,1,0:T(8,128)(2,1)}), bf16[16,32,16,128]{3,2,1,0:T(8,128)(2,1)S(1)}, u32[]{:S(2)}, u32[]{:S(2)}) async-start(bf16[16,32,16,128]{3,2,1,0:T(8,128)(2,1)} %bitcast.287), calls=%async_computation.1 | async-start | bytes 4194304 | tf_op jit(solution)/shard_map/all_to_all | solution.py:114
  281.8 14.8 %all-to-all-start.2 = ((bf16[32,16,128]{2,1,0:T(8,128)(2,1)}), bf16[32,16,128]{2,1,0:T(8,128)(2,1)S(1)}, u32[]{:S(2)}, u32[]{:S(2)}) async-start(bf16[32,16,128]{2,1,0:T(8,128)(2,1)} %reduce_sum.69), calls=%async_computation.2 | async-start | bytes 262144 | tf_op jit(solution)/shard_map/all_to_all | solution.py:281
  (5 other events, 43.9 us)
